TPU v7x, 256 devices: a whole 4x4x8 slice. The times are simulated.
256 devices in a mesh: sp: 64 (over z, x, core), tp: 4 (over y).
Axes of the slice: x: 4, y: 4, z: 8, core: 2. Of those that a mesh axis runs over, the one named last changes fastest.
Arguments:
- stream_in: bfloat16 [16384, 2048], P(('sp', 'tp')), may hold values from -6 to 6
- queries: bfloat16 [16384, 1024], P('sp', 'tp'), may hold values from -48 to 48
- keys: bfloat16 [16384, 512], P('sp', 'tp'), may hold values from -48 to 48
- values: bfloat16 [16384, 512], P('sp', 'tp'), may hold values from -6 to 6
- query_gain: float32 [64], replicated, may hold values from 1.5 to 6
- key_gain: float32 [64], replicated, may hold values from 1.5 to 6
- out_rows: bfloat16 [1024, 2048], P('tp'), may hold values from -0.1875 to 0.1875
- norm_gain: float32 [2048], replicated, may hold values from 0.1 to 1.9
- route_ids: int32 [16384, 2], P(('sp', 'tp')), may hold values from 0 to 63, all different within a row; in each aligned block of 64 rows (0 to 63, 64 to 127, ...) at most 3 rows name the same one
- route_weights: float32 [16384, 2], P(('sp', 'tp')), may hold values from 0.25 to 1
- gate_weight: bfloat16 [64, 2048, 3072], P('sp', None, 'tp'), may hold values from -0.125 to 0.125
- up_weight: bfloat16 [64, 2048, 3072], P('sp', None, 'tp'), may hold values from -0.125 to 0.125
- down_weight: bfloat16 [64, 3072, 2048], P('sp', 'tp'), may hold values from -0.109375 to 0.109375
Outputs:
- stream_out: bfloat16 [16384, 2048], P(('sp', 'tp'))
Inputs may be any that keep to these rules, and one draw needn't show every extreme that they name: `route_ids`: each row names 2 different experts; among the rows of one device no expert is named more than 3 times.
All inputs are finite; a program needn't handle non-finite values.
Results may differ from a plain program's by a relative error of at most 0.014.
The roundings to bfloat16 on the way count: a program that leaves them out, or rounds other values in their place, can miss the bound.
Values may be sent and summed in bfloat16 or wider, within the bound.
A program may use at most 128 MiB of HBM per device.

v0:
```python
import math
import jax
import jax.numpy as jnp
from jax import lax
from jax.sharding import PartitionSpec as P

GRID_W = 64
EPS = 1e-06
THETA = 10000.0


def partner(x, axis, distance):
    return lax.ppermute(x, axis, [(i, i ^ 1 << distance) for i in range(lax.axis_size(axis))])


def grouped_exchange(x, axis, split_dim, concat_dim, work, item_dim, out_dim):
    items = jax.tree.leaves(x)[0].shape[item_dim]
    count = 2 if items % 2 == 0 else 1
    outs = []
    for k in range(count):
        group = jax.tree.map(
            lambda a: lax.slice_in_dim(
                a, k * (items // count), (k + 1) * (items // count), axis=item_dim
            ),
            x,
        )
        outs.append(
            work(
                lax.all_to_all(
                    group, axis, split_axis=split_dim, concat_axis=concat_dim, tiled=True
                )
            )
        )
    return jax.tree.map(lambda *parts: jnp.concatenate(parts, axis=out_dim), *outs)


def turn_tables(offset, count, head_size):
    position = offset + jnp.arange(count, dtype=jnp.int32)
    grid_row = (position // GRID_W).astype(jnp.float32)
    column = (position % GRID_W).astype(jnp.float32)
    pair_index = jnp.arange(head_size // 4, dtype=jnp.float32)
    inverse = THETA ** (-4.0 * pair_index / head_size)
    angles = jnp.concatenate([grid_row[:, None] * inverse, column[:, None] * inverse], axis=1)
    return (jnp.cos(angles), jnp.sin(angles))


def normalize_rotate(block_data, gain_vector, cos_table, sin_table):
    row_count = block_data.shape[0]
    head_size = gain_vector.shape[0]
    wide = block_data.astype(jnp.float32).reshape(row_count, -1, head_size)
    wide = wide * lax.rsqrt(jnp.mean(wide * wide, axis=-1, keepdims=True) + EPS) * gain_vector
    pairs = wide.reshape(row_count, wide.shape[1], head_size // 2, 2)
    even_part = pairs[..., 0]
    odd_part = pairs[..., 1]
    cosine = cos_table[:, None, :]
    sine_part = sin_table[:, None, :]
    turned = jnp.stack(
        [even_part * cosine - odd_part * sine_part, even_part * sine_part + odd_part * cosine],
        axis=-1,
    )
    return turned.reshape(row_count, -1).astype(jnp.bfloat16)


def local(
    stream_in,
    queries,
    keys,
    values,
    query_gain,
    key_gain,
    out_rows,
    norm_gain,
    route_ids,
    route_weights,
    gate_weight,
    up_weight,
    down_weight,
):
    head_size = query_gain.shape[0]
    seq_rows = queries.shape[0]
    query_heads = queries.shape[1] // head_size
    key_heads = keys.shape[1] // head_size
    group_head_count = query_heads // key_heads
    whole_out = lax.all_gather(out_rows, "tp", axis=0, tiled=True)
    place_in_seq = lax.axis_index("sp")
    cos_table, sin_table = turn_tables(place_in_seq * seq_rows, seq_rows, head_size)
    rotated_queries = normalize_rotate(queries, query_gain, cos_table, sin_table).reshape(
        seq_rows, key_heads, group_head_count, head_size
    )
    rotated_keys = normalize_rotate(keys, key_gain, cos_table, sin_table)
    score_scale = head_size ** (-0.5)

    def absorb(carry, pieces):
        key_piece, value_piece = pieces
        sequence_length = key_piece.shape[0]
        span_rows = math.gcd(sequence_length, 4 * seq_rows)
        block_count = sequence_length // span_rows
        key_blocks = key_piece.reshape(block_count, span_rows, key_heads, head_size)
        value_blocks = value_piece.reshape(block_count, span_rows, key_heads, head_size)

        def one_block(running, blocks_pair):
            row_top, row_total, weighted = running
            key_block, value_block = blocks_pair
            scores = (
                jnp.einsum(
                    "qkgd,skd->qkgs", rotated_queries, key_block, preferred_element_type=jnp.float32
                )
                * score_scale
            )
            new_top = jnp.maximum(row_top, jnp.max(scores, axis=-1))
            weights = jnp.exp(scores - new_top[..., None])
            shrink = jnp.exp(row_top - new_top)
            row_total = row_total * shrink + jnp.sum(weights, axis=-1)
            weighted = weighted * shrink[..., None] + jnp.einsum(
                "qkgs,skd->qkgd",
                weights.astype(jnp.bfloat16),
                value_block,
                preferred_element_type=jnp.float32,
            )
            return ((new_top, row_total, weighted), None)

        return lax.scan(one_block, carry, (key_blocks, value_blocks))[0]

    start_top = jnp.full((seq_rows, key_heads, group_head_count), -1e30, jnp.float32)
    start_total = jnp.zeros((seq_rows, key_heads, group_head_count), jnp.float32)
    start_weighted = jnp.zeros((seq_rows, key_heads, group_head_count, head_size), jnp.float32)
    carried = absorb((start_top, start_total, start_weighted), (rotated_keys, values))
    held_keys = rotated_keys
    held_values = values
    level_count = lax.axis_size("sp").bit_length() - 1
    for bit in range(level_count):
        partner_keys, partner_values = partner((held_keys, held_values), "sp", bit)
        carried = absorb(carried, (partner_keys, partner_values))
        if bit + 1 < level_count:
            held_keys = jnp.concatenate([held_keys, partner_keys], axis=0)
            held_values = jnp.concatenate([held_values, partner_values], axis=0)
    row_top, row_total, weighted = carried
    attended = (
        (weighted / row_total[..., None])
        .astype(jnp.bfloat16)
        .reshape(seq_rows, query_heads * head_size)
    )
    token_heads = lax.all_to_all(attended, "tp", split_axis=0, concat_axis=1, tiled=True)
    projected = jnp.dot(token_heads, whole_out, preferred_element_type=jnp.float32)
    stream = (stream_in.astype(jnp.float32) + projected).astype(jnp.bfloat16)
    stream_wide = stream.astype(jnp.float32)
    normed = (
        stream_wide
        * lax.rsqrt(jnp.mean(stream_wide * stream_wide, axis=1, keepdims=True) + EPS)
        * norm_gain
    ).astype(jnp.bfloat16)
    tokens = stream.shape[0]
    model_width = stream.shape[1]
    top_count = route_ids.shape[1]
    experts = lax.axis_size("sp")
    routed = tokens * top_count
    capacity = max(2, (5 * routed + 4 * experts - 1) // (4 * experts))
    flat_ids = route_ids.reshape(routed)
    member = (flat_ids[:, None] == jnp.arange(experts, dtype=jnp.int32)[None, :]).astype(jnp.int32)
    earlier = jnp.cumsum(member, axis=0) - member
    slot_rank = jnp.sum(earlier * member, axis=1)
    target = flat_ids * capacity + slot_rank
    placed = (target[:, None] == jnp.arange(experts * capacity, dtype=jnp.int32)[None, :]).astype(
        jnp.bfloat16
    )
    placed = placed.reshape(tokens, top_count, experts * capacity)
    outgoing = jnp.einsum("tks,td->sd", placed, normed, preferred_element_type=jnp.float32).astype(
        jnp.bfloat16
    )
    outgoing = outgoing.reshape(experts, capacity, model_width)
    gate_shard = gate_weight[0]
    up_shard = up_weight[0]
    down_shard = down_weight[0]

    def expert_work(arrived):
        sources, slot_count, width_here = arrived.shape
        flat_rows = arrived.reshape(sources * slot_count, width_here)
        row_piece = lax.all_gather(flat_rows, "tp", axis=0, tiled=True)
        gate_value = jnp.dot(row_piece, gate_shard, preferred_element_type=jnp.float32)
        up_value = jnp.dot(row_piece, up_shard, preferred_element_type=jnp.float32)
        hidden = (jax.nn.silu(gate_value) * up_value).astype(jnp.bfloat16)
        summed = lax.psum_scatter(
            jnp.dot(
                lax.slice_in_dim(hidden, 0, sources * slot_count * lax.axis_size("tp"), axis=0),
                down_shard,
                preferred_element_type=jnp.float32,
            ).astype(jnp.bfloat16),
            "tp",
            scatter_dimension=0,
            tiled=True,
        )
        answer = summed.reshape(sources, slot_count, width_here)
        return lax.all_to_all(answer, "sp", split_axis=0, concat_axis=0, tiled=True)

    returned = grouped_exchange(outgoing, "sp", 0, 0, expert_work, 1, 1)
    expert_back = returned.reshape(experts * capacity, model_width)
    picked = jnp.einsum("tks,sd->tkd", placed, expert_back, preferred_element_type=jnp.float32)
    mixed_out = stream_wide + jnp.sum(route_weights[:, :, None] * picked, axis=1)
    return mixed_out.astype(jnp.bfloat16)


def solution(mesh):
    return jax.shard_map(
        local,
        mesh=mesh,
        in_specs=(
            P(("sp", "tp"), None),
            P("sp", "tp"),
            P("sp", "tp"),
            P("sp", "tp"),
            P(),
            P(),
            P("tp", None),
            P(),
            P(("sp", "tp"), None),
            P(("sp", "tp"), None),
            P("sp", None, "tp"),
            P("sp", None, "tp"),
            P("sp", "tp", None),
        ),
        out_specs=P(("sp", "tp"), None),
        check_vma=False,
    )
```

profile of v0, /device:TPU:1, one launch (start us, length us, event | category | flops | bytes accessed | tf_op | source)
XLA Modules:
  0.0 646.2 jit_solution(744757202785638066)
XLA Ops:
  9.6 3.3 collective-permute-start
  23.6 2.3 fusion.122
  41.1 1.9 collective-permute-start.5
  49.4 1.8 bitcast_reduce_fusion.3
  51.2 2.2 pad_maximum_fusion
  54.4 1.8 pad_maximum_fusion.1
  56.2 1.9 collective-permute-start.7
  60.5 1.9 constant_dynamic-update-slice_fusion.12
  64.1 3.1 fusion.80
  67.2 2.2 reshape.298
  69.5 2.0 copy.102
  71.5 5.5 collective-permute-done.7
  77.0 3.2 reshape.324
  80.1 3.5 copy.103
  83.7 2.1 constant_dynamic-update-slice_fusion.11
  87.4 2.2 constant_dynamic-update-slice_fusion.17
  90.3 7.3 %while.6 = (s32[]{:T(128)}, f32[256,2,2]{0,2,1:T(2,128)S(1)}, f32[256,2,2]{0,2,1:T(2,128)S(1)}, f32[256,2,2,64]{0,3,2,1:T(8,128)S(1)}, bf16[2,1024,2,64]{1,3,2,0...) while((s32[]{:T(128)}, f32[256,2,2]{0,2,1:T(2,128)S(1)}, ...), condition=%wide.region_13.14_spmd, body=%wide.region_10.13_spmd.sunk | while | flops 276957184 | bytes 15925377 | solution.py:122
  94.0 1.7 bitcast_reduce_fusion.10
  97.6 59.1 %collective-permute-done.8 = bf16[4096,128]{0,1:T(8,128)(2,1)} collective-permute-done((bf16[4096,128]{0,1:T(8,128)(2,1)}, bf16[4096,128]{0,1:T(8,128)(2,1)}, u32[]{:S(2)}, u32[]{:S(2)}) %collective-permute-start.8) | collective-permute-done | bytes 1048608 | tf_op jit(solution)/shard_map/ppermute | solution.py:13
  156.8 2.6 reshape.300
  159.4 2.5 copy.105
  161.9 17.3 %collective-permute-done.9 = bf16[4096,128]{1,0:T(8,128)(2,1)} collective-permute-done((bf16[4096,128]{1,0:T(8,128)(2,1)}, bf16[4096,128]{1,0:T(8,128)(2,1)}, u32[]{:S(2)}, u32[]{:S(2)}) %collective-permute-start.9) | collective-permute-done | bytes 1048608 | tf_op jit(solution)/shard_map/ppermute | solution.py:13
  179.2 5.0 reshape.325
  184.2 5.9 copy.106
  190.1 2.3 constant_dynamic-update-slice_fusion.10
  192.4 5.0 collective-permute-start.10
  197.4 2.3 constant_dynamic-update-slice_fusion.16
  200.2 17.3 %while.7 = (s32[]{:T(128)}, f32[256,2,2]{0,2,1:T(2,128)S(1)}, f32[256,2,2]{0,2,1:T(2,128)S(1)}, f32[256,2,2,64]{0,3,2,1:T(8,128)S(1)}, bf16[4,1024,2,64]{1,3,2,0...) while((s32[]{:T(128)}, f32[256,2,2]{0,2,1:T(2,128)S(1)}, ...), condition=%wide.region_17.18_spmd, body=%wide.region_14.17_spmd.sunk | while | flops 276957184 | bytes 13828197 | solution.py:122
  202.7 1.8 fusion.167
  207.0 1.8 fusion.167
  211.3 1.8 fusion.167
  213.1 1.7 bitcast_reduce_fusion.11
  215.6 1.8 fusion.167
  217.5 94.2 %collective-permute-done.10 = bf16[8192,128]{0,1:T(8,128)(2,1)} collective-permute-done((bf16[8192,128]{0,1:T(8,128)(2,1)}, bf16[8192,128]{0,1:T(8,128)(2,1)}, u32[]{:S(2)}, u32[]{:S(2)}) %collective-permute-start.10) | collective-permute-done | bytes 2097184 | tf_op jit(solution)/shard_map/ppermute | solution.py:13
  311.7 3.0 copy.143
  314.7 2.5 copy.108
  317.2 61.5 %collective-permute-done.11 = bf16[8192,128]{1,0:T(8,128)(2,1)} collective-permute-done((bf16[8192,128]{1,0:T(8,128)(2,1)}, bf16[8192,128]{1,0:T(8,128)(2,1)}, u32[]{:S(2)}, u32[]{:S(2)}) %collective-permute-start.11) | collective-permute-done | bytes 2097184 | tf_op jit(solution)/shard_map/ppermute | solution.py:13
  378.6 8.3 %reshape.326 = bf16[8,1024,2,64]{3,2,1,0:T(2,128)(2,1)} reshape(bf16[8192,128]{1,0:T(8,128)(2,1)} %collective-permute-done.11) | data formatting | bytes 4194304 | tf_op jit(solution)/shard_map/reshape | solution.py:99
  386.9 10.7 %copy.109 = bf16[8,1024,2,64]{1,3,2,0:T(8,128)(2,1)} copy(bf16[8,1024,2,64]{3,2,1,0:T(2,128)(2,1)} %reshape.326) | data formatting | bytes 4194304 | tf_op jit(solution)/shard_map/while | solution.py:122
  397.5 34.5 %while.8 = (s32[]{:T(128)}, f32[256,2,2]{0,2,1:T(2,128)S(1)}, f32[256,2,2]{0,2,1:T(2,128)S(1)}, f32[256,2,2,64]{0,3,2,1:T(8,128)S(1)}, bf16[8,1024,2,64]{1,3,2,0...) while((s32[]{:T(128)}, f32[256,2,2]{0,2,1:T(2,128)S(1)}, ...), condition=%wide.region_21.22_spmd, body=%wide.region_18.21_spmd.sunk | while | flops 276957184 | bytes 13828197 | solution.py:122
  400.0 1.8 fusion.172
  404.3 1.8 fusion.172
  408.6 1.8 fusion.172
  410.5 1.7 bitcast_reduce_fusion.12
  413.0 1.8 fusion.172
  414.8 1.7 bitcast_reduce_fusion.12
  417.3 1.8 fusion.172
  421.6 1.8 fusion.172
  425.9 1.8 fusion.172
  430.2 1.8 fusion.172
  434.7 4.0 all-to-all-start
  438.7 4.7 all-to-all-done
  443.5 3.2 multiply_reduce_fusion
  448.9 3.3 reshape.304
  452.2 38.9 %all_to_all.29 = bf16[64,3,2048]{2,1,0:T(4,128)(2,1)} all-to-all(bf16[64,3,2048]{2,1,0:T(4,128)(2,1)} %reshape.304), channel_id=1, replica_groups=mesh['sp'=64,'tp'=4] {'sp'}, dimensions={0} | all-to-all | bytes 1572864 | tf_op jit(solution)/shard_map/all_to_all | solution.py:29
  491.1 3.2 reshape.305
  494.4 37.1 %all-gather.5.cloned.1.call-done = bf16[768,2048]{1,0:T(8,128)(2,1)} async-done(((bf16[192,2048]{1,0:T(8,128)(2,1)}), bf16[768,2048]{1,0:T(8,128)(2,1)}) %all-gather.5.cloned.1.call-update) | async-done | bytes 3145744 | tf_op jit(solution)/shard_map/all_gather | solution.py:178
  531.4 6.9 %fusion.61 = f32[768,768]{1,0:T(8,128)} fusion(bf16[768,2048]{1,0:T(8,128)(2,1)} %all-gather.5.cloned.1.call-done, bf16[1,2048,768]{2,1,0:T(8,128)(2,1)} %param.30), kind=kOutput, calls=%fused_computation.61 | convolution fusion | flops 2415919104 | bytes 8650752 | tf_op jit(solution)/shard_map/dot_general | solution.py:180
  538.3 11.0 %convolution_convert_fusion = bf16[768,2048]{1,0:T(8,128)(2,1)} fusion(bf16[1,768,2048]{2,1,0:T(8,128)(2,1)S(1)} %copy-done, f32[768,768]{1,0:T(8,128)} %fusion.61, bf16[768,2048]{1,0:T(8,128)(2,1)} %all-gather.5.cloned.1.call-done, bf16[1,2048,768]{2,1,0:T(8,128)(2,1)} %param.29), kind=kOutput, calls=%fused_computation.59 | convolution fusion | flops 4836950016 | bytes 14942208 | tf_op jit(solution)/shard_map/dot_general | solution.py:183
  549.4 41.3 %reduce-scatter.2.cloned.1.call-done = bf16[192,2048]{1,0:T(8,128)(2,1)} async-done(((bf16[768,2048]{1,0:T(8,128)(2,1)}), bf16[192,2048]{1,0:T(8,128)(2,1)}) %reduce-scatter.2.cloned.1.call-update) | async-done | bytes 786448 | tf_op jit(solution)/shard_map/reduce_scatter | solution.py:182
  590.7 3.3 reshape.306
  593.9 39.0 %all_to_all.30 = bf16[64,3,2048]{2,1,0:T(4,128)(2,1)} all-to-all(bf16[64,3,2048]{2,1,0:T(4,128)(2,1)} %reshape.306), channel_id=1, replica_groups=mesh['sp'=64,'tp'=4] {'sp'}, dimensions={0} | all-to-all | bytes 1572864 | tf_op jit(solution)/shard_map/all_to_all | solution.py:193
  632.9 3.2 reshape.322
  637.6 1.8 add_convert_fusion
  (207 shorter events, 79.2 us)
Async XLA Ops:
  6.5 531.8 %copy-start = (bf16[1,768,2048]{2,1,0:T(8,128)(2,1)S(1)}, bf16[1,768,2048]{2,1,0:T(8,128)(2,1)}, u32[]{:S(2)}) copy-start(bf16[1,768,2048]{2,1,0:T(8,128)(2,1)} %param.31) | copy-start | bytes 9437188
  6.5 9.1 %copy-start.12 = (bf16[256,128]{1,0:T(8,128)(2,1)S(1)}, bf16[256,128]{1,0:T(8,128)(2,1)}, u32[]{:S(2)}) copy-start(bf16[256,128]{1,0:T(8,128)(2,1)} %param.22) | copy-start | bytes 196612
  6.5 10.5 %copy-start.24 = (f32[64]{0:T(128)S(1)}, f32[64]{0:T(128)}, u32[]{:S(2)}) copy-start(f32[64]{0:T(128)} %param.23) | copy-start | bytes 772
  6.5 14.7 %copy-start.22 = (s32[64,2]{0,1:T(2,128)S(1)}, s32[64,2]{0,1:T(2,128)}, u32[]{:S(2)}) copy-start(s32[64,2]{0,1:T(2,128)} %param.27) | copy-start | bytes 1540
  6.5 437.0 %all-gather.3.cloned.1.call-start = ((), (), s32[]{:S(2)}) async-start(), calls=%async_computation.4 | async-start | bytes 5242880 | tf_op jit(solution)/shard_map/all_gather | solution.py:84
  8.8 0.6 copy-start.17
  8.8 0.6 copy-start.18
  9.6 16.9 %copy-start.14 = (bf16[256,128]{0,1:T(8,128)(2,1)}, bf16[256,128]{0,1:T(8,128)(2,1)S(1)}, u32[]{:S(2)}) copy-start(bf16[256,128]{0,1:T(8,128)(2,1)S(1)} %convert_element_type.105) | copy-start | bytes 196612
  9.6 16.9 %collective-permute-start = (bf16[256,128]{0,1:T(8,128)(2,1)S(1)}, bf16[256,128]{0,1:T(8,128)(2,1)S(1)}, u32[]{:S(2)}, u32[]{:S(2)}) collective-permute-start(bf16[256,128]{0,1:T(8,128)(2,1)S(1)} %convert_element_type.105), channel_id=1, source_target_pairs={{0,4},{4,0},{8,12},{12,8},{16,20},{20,16},{24,28},{28,24},{32,36},... | collective-permute-start | bytes 196616 | tf_op jit(solution)/shard_map/ppermute | solution.py:13
  12.9 15.6 %collective-permute-start.3 = (bf16[256,128]{1,0:T(8,128)(2,1)}, bf16[256,128]{1,0:T(8,128)(2,1)}, u32[]{:S(2)}, u32[]{:S(2)}) collective-permute-start(bf16[256,128]{1,0:T(8,128)(2,1)} %param.22), channel_id=1, source_target_pairs={{0,4},{4,0},{8,12},{12,8},{16,20},{20,16},{24,28},{28,24},{32,36},... | collective-permute-start | bytes 196616 | tf_op jit(solution)/shard_map/ppermute | solution.py:13
  26.6 2.0 copy-start.10
  27.2 8.9 %collective-permute-start.1 = (bf16[512,128]{0,1:T(8,128)(2,1)}, bf16[512,128]{0,1:T(8,128)(2,1)S(1)}, u32[]{:S(2)}, u32[]{:S(2)}) collective-permute-start(bf16[512,128]{0,1:T(8,128)(2,1)} %pad_maximum_fusion.5), channel_id=1, source_target_pairs={{0,8},{4,12},{8,0},{12,4},{16,24},{20,28},{24,16},{28,20},{32,40},... | collective-permute-start | bytes 393224 | tf_op jit(solution)/shard_map/ppermute | solution.py:13
  30.1 8.8 %collective-permute-start.4 = (bf16[512,128]{1,0:T(8,128)(2,1)}, bf16[512,128]{1,0:T(8,128)(2,1)S(1)}, u32[]{:S(2)}, u32[]{:S(2)}) collective-permute-start(bf16[512,128]{1,0:T(8,128)(2,1)} %pad_maximum_fusion.6), channel_id=1, source_target_pairs={{0,8},{4,12},{8,0},{12,4},{16,24},{20,28},{24,16},{28,20},{32,40},... | collective-permute-start | bytes 393224 | tf_op jit(solution)/shard_map/ppermute | solution.py:13
  36.1 2.7 copy-start.6
  37.8 11.6 %collective-permute-start.2 = (bf16[1024,128]{0,1:T(8,128)(2,1)}, bf16[1024,128]{0,1:T(8,128)(2,1)}, u32[]{:S(2)}, u32[]{:S(2)}) collective-permute-start(bf16[1024,128]{0,1:T(8,128)(2,1)} %pad_maximum_fusion.2), channel_id=1, source_target_pairs={{0,16},{4,20},{8,24},{12,28},{16,0},{20,4},{24,8},{28,12},{32,48},... | collective-permute-start | bytes 786440 | tf_op jit(solution)/shard_map/ppermute | solution.py:13
  38.8 0.7 copy-start.8
  41.1 13.3 %collective-permute-start.5 = (bf16[1024,128]{1,0:T(8,128)(2,1)}, bf16[1024,128]{1,0:T(8,128)(2,1)S(1)}, u32[]{:S(2)}, u32[]{:S(2)}) collective-permute-start(bf16[1024,128]{1,0:T(8,128)(2,1)} %pad_maximum_fusion.3), channel_id=1, source_target_pairs={{0,16},{4,20},{8,24},{12,28},{16,0},{20,4},{24,8},{28,12},{32,48},... | collective-permute-start | bytes 786440 | tf_op jit(solution)/shard_map/ppermute | solution.py:13
  47.9 3.3 copy-start.7
  47.9 3.3 copy-start.11
  47.9 3.3 copy-start.15
  49.4 4.4 copy-start.16
  51.2 6.9 %copy-start.1 = (f32[2,1024,256,2]{2,1,3,0:T(8,128)}, f32[2,1024,256,2]{2,1,3,0:T(8,128)S(1)}, u32[]{:S(2)}) copy-start(f32[2,1024,256,2]{2,1,3,0:T(8,128)S(1)} %get-tuple-element.368) | copy-start | bytes 12582916
  51.2 3.1 copy-start.9
  51.2 3.1 copy-start.13
  53.4 13.8 %collective-permute-start.6 = (bf16[2048,128]{0,1:T(8,128)(2,1)}, bf16[2048,128]{0,1:T(8,128)(2,1)}, u32[]{:S(2)}, u32[]{:S(2)}) collective-permute-start(bf16[2048,128]{0,1:T(8,128)(2,1)} %pad_maximum_fusion), channel_id=1, source_target_pairs={{0,32},{4,36},{8,40},{12,44},{16,48},{20,52},{24,56},{28,60},{32,0... | collective-permute-start | bytes 1572872 | tf_op jit(solution)/shard_map/ppermute | solution.py:13
  54.3 4.5 copy-start.3
  54.3 4.6 copy-start.2
  56.2 20.8 %collective-permute-start.7 = (bf16[2048,128]{1,0:T(8,128)(2,1)}, bf16[2048,128]{1,0:T(8,128)(2,1)}, u32[]{:S(2)}, u32[]{:S(2)}) collective-permute-start(bf16[2048,128]{1,0:T(8,128)(2,1)} %pad_maximum_fusion.1), channel_id=1, source_target_pairs={{0,32},{4,36},{8,40},{12,44},{16,48},{20,52},{24,56},{28,60},{32,0... | collective-permute-start | bytes 1572872 | tf_op jit(solution)/shard_map/ppermute | solution.py:13
  58.1 1.1 copy-start.19
  58.1 1.4 copy-start.20
  85.8 71.0 %collective-permute-start.8 = (bf16[4096,128]{0,1:T(8,128)(2,1)}, bf16[4096,128]{0,1:T(8,128)(2,1)}, u32[]{:S(2)}, u32[]{:S(2)}) collective-permute-start(bf16[4096,128]{0,1:T(8,128)(2,1)} %get-tuple-element.340), channel_id=1, source_target_pairs={{0,64},{4,68},{8,72},{12,76},{16,80},{20,84},{24,88},{28,92},{32,9... | collective-permute-start | bytes 3145736 | tf_op jit(solution)/shard_map/ppermute | solution.py:13
  89.6 89.7 %collective-permute-start.9 = (bf16[4096,128]{1,0:T(8,128)(2,1)}, bf16[4096,128]{1,0:T(8,128)(2,1)}, u32[]{:S(2)}, u32[]{:S(2)}) collective-permute-start(bf16[4096,128]{1,0:T(8,128)(2,1)} %get-tuple-element.338), channel_id=1, source_target_pairs={{0,64},{4,68},{8,72},{12,76},{16,80},{20,84},{24,88},{28,92},{32,9... | collective-permute-start | bytes 3145736 | tf_op jit(solution)/shard_map/ppermute | solution.py:13
  92.1 1.0 copy-start.4
  95.7 1.0 copy-start.4
  192.4 119.3 %collective-permute-start.10 = (bf16[8192,128]{0,1:T(8,128)(2,1)}, bf16[8192,128]{0,1:T(8,128)(2,1)}, u32[]{:S(2)}, u32[]{:S(2)}) collective-permute-start(bf16[8192,128]{0,1:T(8,128)(2,1)} %constant_dynamic-update-slice_fusion.10), channel_id=1, source_target_pairs={{0,128},{4,132},{8,136},{12,140},{16,144},{20,148},{24,152},{28,15... | collective-permute-start | bytes 6291464 | tf_op jit(solution)/shard_map/ppermute | solution.py:13
  199.7 178.9 %collective-permute-start.11 = (bf16[8192,128]{1,0:T(8,128)(2,1)}, bf16[8192,128]{1,0:T(8,128)(2,1)}, u32[]{:S(2)}, u32[]{:S(2)}) collective-permute-start(bf16[8192,128]{1,0:T(8,128)(2,1)} %constant_dynamic-update-slice_fusion.16), channel_id=1, source_target_pairs={{0,128},{4,132},{8,136},{12,140},{16,144},{20,148},{24,152},{28,15... | collective-permute-start | bytes 6291464 | tf_op jit(solution)/shard_map/ppermute | solution.py:13
  432.8 14.8 %copy-start.21 = (f32[2048]{0:T(1024)S(1)}, f32[2048]{0:T(1024)}, u32[]{:S(2)}) copy-start(f32[2048]{0:T(1024)} %param.26) | copy-start | bytes 24580
  434.7 8.8 %all-to-all-start = ((bf16[4,64,256]{2,1,0:T(8,128)(2,1)}), bf16[4,64,256]{2,1,0:T(8,128)(2,1)S(1)}, u32[]{:S(2)}, u32[]{:S(2)}) async-start(bf16[4,64,256]{2,1,0:T(8,128)(2,1)} %copy.141), calls=%async_computation | async-start | bytes 262144 | tf_op jit(solution)/shard_map/all_to_all | solution.py:143
  438.6 92.8 %all-gather.5.cloned.1.call-start = ((), (), s32[]{:S(2)}) async-start(), calls=%async_computation.5 | async-start | bytes 3932160 | tf_op jit(solution)/shard_map/all_gather | solution.py:178
  446.7 0.9 copy-start.5
  494.3 96.3 %reduce-scatter.2.cloned.1.call-start = ((), (), s32[]{:S(2)}) async-start(), calls=%async_computation.6 | async-start | bytes 3932160 | tf_op jit(solution)/shard_map/reduce_scatter | solution.py:182
  549.4 86.8 %copy-start.23 = (f32[64,2]{0,1:T(2,128)S(1)}, f32[64,2]{0,1:T(2,128)}, u32[]{:S(2)}) copy-start(f32[64,2]{0,1:T(2,128)} %param.28) | copy-start | bytes 1540
Sparse Core Ops, SparseCore 0:
  13.2 51.5 all-gather.2
  494.4 36.9 all-gather.4
  549.5 41.1 reduce-scatter.1
where the time goes:
time: 657 us; the launch traced here: 646 us
  waiting for transfers between devices  321 us (49%)
  local copies, waits for them, and re-layouts  98.7 us (15%)
  matrix products  83.3 us (13%)
  blocking collectives  77.9 us (12%)
  other arithmetic  29.4 us (4%)
  starting transfers between devices  21.7 us (3%)
  between operations  13.8 us (2%)
    ppermute x12, waiting for transfers between devices, partner(): lax.ppermute(x, axis, [(i, i ^ 1 << distance) for i in range(lax.axis_siz...  238 us
    reduce_scatter x1, waiting for transfers between devices, expert_work(): lax.psum_scatter(jnp.dot(lax.slice_in_dim(hidden, 0, sources * slot_count...  41.3 us
    all_to_all x1, blocking collectives, expert_work(): return lax.all_to_all(answer, 'sp', split_axis=0, concat_axis=0, tiled=True)  39 us
    all_to_all x1, blocking collectives, grouped_exchange(): lax.all_to_all(group, axis, split_axis=split_dim, concat_axis=concat_dim,...  38.9 us
    all_gather x1, waiting for transfers between devices, expert_work(): row_piece = lax.all_gather(flat_rows, 'tp', axis=0, tiled=True)  37.1 us
    dot_general x18, matrix products, one_block(): jnp.einsum('qkgd,skd->qkgs', rotated_queries, key_block, preferred_elemen...  30.8 us
    dot_general x18, matrix products, one_block(): jnp.einsum('qkgs,skd->qkgd', weights.astype(jnp.bfloat16), value_block, p...  28.5 us
    while x6, local copies, waits for them, and re-layouts, absorb(): return lax.scan(one_block, carry, (key_blocks, value_blocks))[0]  27.1 us
  transfers between devices with their start and end apart: 16, of which 8 were waited for; matrix products, arithmetic and copies ran while one was open for 26% of the time, Pallas kernels for 0%

commit v1 on v0

--- a/solution.py
+++ b/solution.py
@@ -175,7 +175,9 @@
     def expert_work(arrived):
         sources, slot_count, width_here = arrived.shape
         flat_rows = arrived.reshape(sources * slot_count, width_here)
-        row_piece = lax.all_gather(flat_rows, "tp", axis=0, tiled=True)
+        row_piece = jnp.concatenate(
+            lax.all_to_all(jnp.stack([flat_rows] * lax.axis_size("tp")), "tp", 0, 0), axis=0
+        )
         gate_value = jnp.dot(row_piece, gate_shard, preferred_element_type=jnp.float32)
         up_value = jnp.dot(row_piece, up_shard, preferred_element_type=jnp.float32)
         hidden = (jax.nn.silu(gate_value) * up_value).astype(jnp.bfloat16)

time: 657 us -> 656 us (level)
  waiting for transfers between devices: 321 us -> 280 us
  blocking collectives: 77.9 us -> 117 us
    all_to_all x0 -> x1, blocking collectives: none -> 39.3 us  [expert_work(): lax.all_to_all(jnp.stack([flat_rows] * lax.axis_size('tp')), 'tp', 0, 0)]
    all_gather x1 -> x0, waiting for transfers between devices: 37.1 us -> none  [expert_work(): row_piece = lax.all_gather(flat_rows, 'tp', axis=0, tiled=True)]
    unnamed x63 -> x67, local copies, waits for them, and re-layouts: 22.5 us -> 24.3 us
  transfers between devices with their start and end apart: 16 -> 15, of which waited for: 8 -> 7; matrix products, arithmetic and copies ran while one was open for 26% -> 26% of each run, Pallas kernels for 0% -> 0%
where the time goes in v1:
time: 656 us; the launch traced here: 645 us
  waiting for transfers between devices  280 us (43%)
  blocking collectives  117 us (18%)
  local copies, waits for them, and re-layouts  102 us (16%)
  matrix products  80.5 us (12%)
  other arithmetic  29.3 us (4%)
  starting transfers between devices  21.6 us (3%)
  between operations  14.1 us (2%)
    ppermute x12, waiting for transfers between devices, partner(): lax.ppermute(x, axis, [(i, i ^ 1 << distance) for i in range(lax.axis_siz...  238 us
    all_to_all x1, blocking collectives, expert_work(): lax.all_to_all(jnp.stack([flat_rows] * lax.axis_size('tp')), 'tp', 0, 0)  39.3 us
    all_to_all x1, blocking collectives, expert_work(): return lax.all_to_all(answer, 'sp', split_axis=0, concat_axis=0, tiled=True)  39 us
    all_to_all x1, blocking collectives, grouped_exchange(): lax.all_to_all(group, axis, split_axis=split_dim, concat_axis=concat_dim,...  38.9 us
    reduce_scatter x1, waiting for transfers between devices, expert_work(): lax.psum_scatter(jnp.dot(lax.slice_in_dim(hidden, 0, sources * slot_count...  37.1 us
    dot_general x18, matrix products, one_block(): jnp.einsum('qkgd,skd->qkgs', rotated_queries, key_block, preferred_elemen...  30.8 us
    dot_general x18, matrix products, one_block(): jnp.einsum('qkgs,skd->qkgd', weights.astype(jnp.bfloat16), value_block, p...  28.5 us
    while x6, local copies, waits for them, and re-layouts, absorb(): return lax.scan(one_block, carry, (key_blocks, value_blocks))[0]  27.1 us
  transfers between devices with their start and end apart: 15, of which 7 were waited for; matrix products, arithmetic and copies ran while one was open for 26% of the time, Pallas kernels for 0%

profile of v1, /device:TPU:1, one launch (start us, length us, event | category | flops | bytes accessed | tf_op | source)
XLA Modules:
  0.0 645.0 jit_solution(7743335574818011838)
XLA Ops:
  9.7 3.3 collective-permute-start
  23.6 2.3 fusion.122
  41.1 1.9 collective-permute-start.5
  49.5 1.8 bitcast_reduce_fusion.3
  51.3 2.2 pad_maximum_fusion
  54.4 1.8 pad_maximum_fusion.1
  56.2 1.9 collective-permute-start.7
  60.5 1.9 constant_dynamic-update-slice_fusion.12
  64.2 3.1 fusion.80
  67.3 2.2 reshape.300
  69.5 2.0 copy.102
  71.5 5.5 collective-permute-done.7
  77.0 3.2 reshape.326
  80.2 3.5 copy.103
  83.7 2.2 constant_dynamic-update-slice_fusion.11
  87.5 2.2 constant_dynamic-update-slice_fusion.17
  90.5 7.3 %while.6 = (s32[]{:T(128)}, f32[256,2,2]{0,2,1:T(2,128)S(1)}, f32[256,2,2]{0,2,1:T(2,128)S(1)}, f32[256,2,2,64]{0,3,2,1:T(8,128)S(1)}, bf16[2,1024,2,64]{1,3,2,0...) while((s32[]{:T(128)}, f32[256,2,2]{0,2,1:T(2,128)S(1)}, ...), condition=%wide.region_13.14_spmd, body=%wide.region_10.13_spmd.sunk | while | flops 276957184 | bytes 15925377 | solution.py:122
  94.1 1.7 bitcast_reduce_fusion.10
  97.8 59.1 %collective-permute-done.8 = bf16[4096,128]{0,1:T(8,128)(2,1)} collective-permute-done((bf16[4096,128]{0,1:T(8,128)(2,1)}, bf16[4096,128]{0,1:T(8,128)(2,1)}, u32[]{:S(2)}, u32[]{:S(2)}) %collective-permute-start.8) | collective-permute-done | bytes 1048608 | tf_op jit(solution)/shard_map/ppermute | solution.py:13
  156.9 2.6 reshape.302
  159.6 2.5 copy.105
  162.1 17.3 %collective-permute-done.9 = bf16[4096,128]{1,0:T(8,128)(2,1)} collective-permute-done((bf16[4096,128]{1,0:T(8,128)(2,1)}, bf16[4096,128]{1,0:T(8,128)(2,1)}, u32[]{:S(2)}, u32[]{:S(2)}) %collective-permute-start.9) | collective-permute-done | bytes 1048608 | tf_op jit(solution)/shard_map/ppermute | solution.py:13
  179.4 5.0 reshape.327
  184.4 5.9 copy.106
  190.3 2.4 constant_dynamic-update-slice_fusion.10
  192.6 5.0 collective-permute-start.10
  197.6 2.3 constant_dynamic-update-slice_fusion.16
  200.4 17.3 %while.7 = (s32[]{:T(128)}, f32[256,2,2]{0,2,1:T(2,128)S(1)}, f32[256,2,2]{0,2,1:T(2,128)S(1)}, f32[256,2,2,64]{0,3,2,1:T(8,128)S(1)}, bf16[4,1024,2,64]{1,3,2,0...) while((s32[]{:T(128)}, f32[256,2,2]{0,2,1:T(2,128)S(1)}, ...), condition=%wide.region_17.18_spmd, body=%wide.region_14.17_spmd.sunk | while | flops 276957184 | bytes 13828197 | solution.py:122
  202.9 1.8 fusion.167
  207.2 1.8 fusion.167
  211.5 1.8 fusion.167
  213.4 1.7 bitcast_reduce_fusion.11
  215.8 1.8 fusion.167
  217.7 94.5 %collective-permute-done.10 = bf16[8192,128]{0,1:T(8,128)(2,1)} collective-permute-done((bf16[8192,128]{0,1:T(8,128)(2,1)}, bf16[8192,128]{0,1:T(8,128)(2,1)}, u32[]{:S(2)}, u32[]{:S(2)}) %collective-permute-start.10) | collective-permute-done | bytes 2097184 | tf_op jit(solution)/shard_map/ppermute | solution.py:13
  312.2 3.0 copy.143
  315.2 2.5 copy.108
  317.7 61.1 %collective-permute-done.11 = bf16[8192,128]{1,0:T(8,128)(2,1)} collective-permute-done((bf16[8192,128]{1,0:T(8,128)(2,1)}, bf16[8192,128]{1,0:T(8,128)(2,1)}, u32[]{:S(2)}, u32[]{:S(2)}) %collective-permute-start.11) | collective-permute-done | bytes 2097184 | tf_op jit(solution)/shard_map/ppermute | solution.py:13
  378.9 8.3 %reshape.328 = bf16[8,1024,2,64]{3,2,1,0:T(2,128)(2,1)} reshape(bf16[8192,128]{1,0:T(8,128)(2,1)} %collective-permute-done.11) | data formatting | bytes 4194304 | tf_op jit(solution)/shard_map/reshape | solution.py:99
  387.1 10.6 %copy.109 = bf16[8,1024,2,64]{1,3,2,0:T(8,128)(2,1)} copy(bf16[8,1024,2,64]{3,2,1,0:T(2,128)(2,1)} %reshape.328) | data formatting | bytes 4194304 | tf_op jit(solution)/shard_map/while | solution.py:122
  397.8 34.5 %while.8 = (s32[]{:T(128)}, f32[256,2,2]{0,2,1:T(2,128)S(1)}, f32[256,2,2]{0,2,1:T(2,128)S(1)}, f32[256,2,2,64]{0,3,2,1:T(8,128)S(1)}, bf16[8,1024,2,64]{1,3,2,0...) while((s32[]{:T(128)}, f32[256,2,2]{0,2,1:T(2,128)S(1)}, ...), condition=%wide.region_21.22_spmd, body=%wide.region_18.21_spmd.sunk | while | flops 276957184 | bytes 13828197 | solution.py:122
  400.2 1.8 fusion.172
  404.5 1.8 fusion.172
  406.4 1.7 bitcast_reduce_fusion.12
  408.9 1.8 fusion.172
  410.7 1.7 bitcast_reduce_fusion.12
  413.2 1.8 fusion.172
  417.5 1.8 fusion.172
  421.8 1.8 fusion.172
  426.1 1.8 fusion.172
  430.5 1.8 fusion.172
  434.9 3.9 all-to-all-start
  438.9 4.7 all-to-all-done
  443.7 3.2 multiply_reduce_fusion
  449.1 3.3 reshape.306
  452.4 38.9 %all_to_all.34 = bf16[64,3,2048]{2,1,0:T(4,128)(2,1)} all-to-all(bf16[64,3,2048]{2,1,0:T(4,128)(2,1)} %reshape.306), channel_id=1, replica_groups=mesh['sp'=64,'tp'=4] {'sp'}, dimensions={0} | all-to-all | bytes 1572864 | tf_op jit(solution)/shard_map/all_to_all | solution.py:29
  491.3 3.2 stack_reshape.2
  496.0 39.3 %all_to_all.35 = bf16[4,192,2048]{2,1,0:T(8,128)(2,1)S(1)} all-to-all(bf16[4,192,2048]{2,1,0:T(8,128)(2,1)S(1)} %stack.16), channel_id=1, replica_groups=mesh['sp'=64,'tp'=4] {'tp'}, dimensions={0} | all-to-all | bytes 6291456 | tf_op jit(solution)/shard_map/all_to_all | solution.py:179
  537.0 4.1 fusion.61
  541.1 11.0 %convolution_convert_fusion = bf16[768,2048]{1,0:T(8,128)(2,1)} fusion(bf16[1,768,2048]{2,1,0:T(8,128)(2,1)S(1)} %copy-done, f32[768,768]{1,0:T(8,128)} %fusion.61, bf16[768,2048]{1,0:T(8,128)(2,1)} %bitcast.297, bf16[1,2048,768]{2,1,0:T(8,128)(2,1)} %param.29), kind=kOutput, calls=%fused_computation.59 | convolution fusion | flops 4836950016 | bytes 14942208 | tf_op jit(solution)/shard_map/dot_general | solution.py:185
  552.1 37.1 %reduce-scatter.2.cloned.1.call-done = bf16[192,2048]{1,0:T(8,128)(2,1)} async-done(((bf16[768,2048]{1,0:T(8,128)(2,1)}), bf16[192,2048]{1,0:T(8,128)(2,1)}) %reduce-scatter.2.cloned.1.call-update) | async-done | bytes 786448 | tf_op jit(solution)/shard_map/reduce_scatter | solution.py:184
  589.2 3.3 reshape.308
  592.5 39.0 %all_to_all.36 = bf16[64,3,2048]{2,1,0:T(4,128)(2,1)} all-to-all(bf16[64,3,2048]{2,1,0:T(4,128)(2,1)} %reshape.308), channel_id=1, replica_groups=mesh['sp'=64,'tp'=4] {'sp'}, dimensions={0} | all-to-all | bytes 1572864 | tf_op jit(solution)/shard_map/all_to_all | solution.py:195
  631.5 3.2 reshape.324
  636.2 1.8 add_convert_fusion
  (210 shorter events, 82.4 us)
Async XLA Ops:
  6.5 534.6 %copy-start = (bf16[1,768,2048]{2,1,0:T(8,128)(2,1)S(1)}, bf16[1,768,2048]{2,1,0:T(8,128)(2,1)}, u32[]{:S(2)}) copy-start(bf16[1,768,2048]{2,1,0:T(8,128)(2,1)} %param.31) | copy-start | bytes 9437188
  6.5 9.1 %copy-start.13 = (bf16[256,128]{1,0:T(8,128)(2,1)S(1)}, bf16[256,128]{1,0:T(8,128)(2,1)}, u32[]{:S(2)}) copy-start(bf16[256,128]{1,0:T(8,128)(2,1)} %param.22) | copy-start | bytes 196612
  6.5 10.5 %copy-start.25 = (f32[64]{0:T(128)S(1)}, f32[64]{0:T(128)}, u32[]{:S(2)}) copy-start(f32[64]{0:T(128)} %param.23) | copy-start | bytes 772
  6.5 14.7 %copy-start.23 = (s32[64,2]{0,1:T(2,128)S(1)}, s32[64,2]{0,1:T(2,128)}, u32[]{:S(2)}) copy-start(s32[64,2]{0,1:T(2,128)} %param.27) | copy-start | bytes 1540
  6.5 437.1 %all-gather.2.cloned.1.call-start = ((), (), s32[]{:S(2)}) async-start(), calls=%async_computation.5 | async-start | bytes 5242880 | tf_op jit(solution)/shard_map/all_gather | solution.py:84
  8.8 0.6 copy-start.18
  8.8 0.6 copy-start.19
  9.6 16.9 %copy-start.15 = (bf16[256,128]{0,1:T(8,128)(2,1)}, bf16[256,128]{0,1:T(8,128)(2,1)S(1)}, u32[]{:S(2)}) copy-start(bf16[256,128]{0,1:T(8,128)(2,1)S(1)} %convert_element_type.105) | copy-start | bytes 196612
  9.7 16.9 %collective-permute-start = (bf16[256,128]{0,1:T(8,128)(2,1)S(1)}, bf16[256,128]{0,1:T(8,128)(2,1)S(1)}, u32[]{:S(2)}, u32[]{:S(2)}) collective-permute-start(bf16[256,128]{0,1:T(8,128)(2,1)S(1)} %convert_element_type.105), channel_id=1, source_target_pairs={{0,4},{4,0},{8,12},{12,8},{16,20},{20,16},{24,28},{28,24},{32,36},... | collective-permute-start | bytes 196616 | tf_op jit(solution)/shard_map/ppermute | solution.py:13
  12.9 15.6 %collective-permute-start.3 = (bf16[256,128]{1,0:T(8,128)(2,1)}, bf16[256,128]{1,0:T(8,128)(2,1)}, u32[]{:S(2)}, u32[]{:S(2)}) collective-permute-start(bf16[256,128]{1,0:T(8,128)(2,1)} %param.22), channel_id=1, source_target_pairs={{0,4},{4,0},{8,12},{12,8},{16,20},{20,16},{24,28},{28,24},{32,36},... | collective-permute-start | bytes 196616 | tf_op jit(solution)/shard_map/ppermute | solution.py:13
  26.6 2.0 copy-start.11
  27.3 8.9 %collective-permute-start.1 = (bf16[512,128]{0,1:T(8,128)(2,1)}, bf16[512,128]{0,1:T(8,128)(2,1)S(1)}, u32[]{:S(2)}, u32[]{:S(2)}) collective-permute-start(bf16[512,128]{0,1:T(8,128)(2,1)} %pad_maximum_fusion.5), channel_id=1, source_target_pairs={{0,8},{4,12},{8,0},{12,4},{16,24},{20,28},{24,16},{28,20},{32,40},... | collective-permute-start | bytes 393224 | tf_op jit(solution)/shard_map/ppermute | solution.py:13
  30.1 8.8 %collective-permute-start.4 = (bf16[512,128]{1,0:T(8,128)(2,1)}, bf16[512,128]{1,0:T(8,128)(2,1)S(1)}, u32[]{:S(2)}, u32[]{:S(2)}) collective-permute-start(bf16[512,128]{1,0:T(8,128)(2,1)} %pad_maximum_fusion.6), channel_id=1, source_target_pairs={{0,8},{4,12},{8,0},{12,4},{16,24},{20,28},{24,16},{28,20},{32,40},... | collective-permute-start | bytes 393224 | tf_op jit(solution)/shard_map/ppermute | solution.py:13
  36.2 2.7 copy-start.7
  37.8 11.6 %collective-permute-start.2 = (bf16[1024,128]{0,1:T(8,128)(2,1)}, bf16[1024,128]{0,1:T(8,128)(2,1)}, u32[]{:S(2)}, u32[]{:S(2)}) collective-permute-start(bf16[1024,128]{0,1:T(8,128)(2,1)} %pad_maximum_fusion.2), channel_id=1, source_target_pairs={{0,16},{4,20},{8,24},{12,28},{16,0},{20,4},{24,8},{28,12},{32,48},... | collective-permute-start | bytes 786440 | tf_op jit(solution)/shard_map/ppermute | solution.py:13
  38.8 0.7 copy-start.9
  41.1 13.3 %collective-permute-start.5 = (bf16[1024,128]{1,0:T(8,128)(2,1)}, bf16[1024,128]{1,0:T(8,128)(2,1)S(1)}, u32[]{:S(2)}, u32[]{:S(2)}) collective-permute-start(bf16[1024,128]{1,0:T(8,128)(2,1)} %pad_maximum_fusion.3), channel_id=1, source_target_pairs={{0,16},{4,20},{8,24},{12,28},{16,0},{20,4},{24,8},{28,12},{32,48},... | collective-permute-start | bytes 786440 | tf_op jit(solution)/shard_map/ppermute | solution.py:13
  48.0 3.3 copy-start.8
  48.0 3.3 copy-start.12
  48.0 3.3 copy-start.16
  49.5 4.4 copy-start.17
  51.2 6.9 %copy-start.1 = (f32[2,1024,256,2]{2,1,3,0:T(8,128)}, f32[2,1024,256,2]{2,1,3,0:T(8,128)S(1)}, u32[]{:S(2)}) copy-start(f32[2,1024,256,2]{2,1,3,0:T(8,128)S(1)} %get-tuple-element.368) | copy-start | bytes 12582916
  51.3 3.1 copy-start.10
  51.3 3.1 copy-start.14
  53.5 13.8 %collective-permute-start.6 = (bf16[2048,128]{0,1:T(8,128)(2,1)}, bf16[2048,128]{0,1:T(8,128)(2,1)}, u32[]{:S(2)}, u32[]{:S(2)}) collective-permute-start(bf16[2048,128]{0,1:T(8,128)(2,1)} %pad_maximum_fusion), channel_id=1, source_target_pairs={{0,32},{4,36},{8,40},{12,44},{16,48},{20,52},{24,56},{28,60},{32,0... | collective-permute-start | bytes 1572872 | tf_op jit(solution)/shard_map/ppermute | solution.py:13
  54.4 4.5 copy-start.3
  54.4 4.7 copy-start.2
  56.2 20.8 %collective-permute-start.7 = (bf16[2048,128]{1,0:T(8,128)(2,1)}, bf16[2048,128]{1,0:T(8,128)(2,1)}, u32[]{:S(2)}, u32[]{:S(2)}) collective-permute-start(bf16[2048,128]{1,0:T(8,128)(2,1)} %pad_maximum_fusion.1), channel_id=1, source_target_pairs={{0,32},{4,36},{8,40},{12,44},{16,48},{20,52},{24,56},{28,60},{32,0... | collective-permute-start | bytes 1572872 | tf_op jit(solution)/shard_map/ppermute | solution.py:13
  58.1 1.1 copy-start.20
  58.1 1.4 copy-start.21
  85.9 71.0 %collective-permute-start.8 = (bf16[4096,128]{0,1:T(8,128)(2,1)}, bf16[4096,128]{0,1:T(8,128)(2,1)}, u32[]{:S(2)}, u32[]{:S(2)}) collective-permute-start(bf16[4096,128]{0,1:T(8,128)(2,1)} %get-tuple-element.340), channel_id=1, source_target_pairs={{0,64},{4,68},{8,72},{12,76},{16,80},{20,84},{24,88},{28,92},{32,9... | collective-permute-start | bytes 3145736 | tf_op jit(solution)/shard_map/ppermute | solution.py:13
  89.7 89.7 %collective-permute-start.9 = (bf16[4096,128]{1,0:T(8,128)(2,1)}, bf16[4096,128]{1,0:T(8,128)(2,1)}, u32[]{:S(2)}, u32[]{:S(2)}) collective-permute-start(bf16[4096,128]{1,0:T(8,128)(2,1)} %get-tuple-element.338), channel_id=1, source_target_pairs={{0,64},{4,68},{8,72},{12,76},{16,80},{20,84},{24,88},{28,92},{32,9... | collective-permute-start | bytes 3145736 | tf_op jit(solution)/shard_map/ppermute | solution.py:13
  92.2 1.0 copy-start.4
  95.9 1.0 copy-start.4
  192.6 119.6 %collective-permute-start.10 = (bf16[8192,128]{0,1:T(8,128)(2,1)}, bf16[8192,128]{0,1:T(8,128)(2,1)}, u32[]{:S(2)}, u32[]{:S(2)}) collective-permute-start(bf16[8192,128]{0,1:T(8,128)(2,1)} %constant_dynamic-update-slice_fusion.10), channel_id=1, source_target_pairs={{0,128},{4,132},{8,136},{12,140},{16,144},{20,148},{24,152},{28,15... | collective-permute-start | bytes 6291464 | tf_op jit(solution)/shard_map/ppermute | solution.py:13
  199.9 178.9 %collective-permute-start.11 = (bf16[8192,128]{1,0:T(8,128)(2,1)}, bf16[8192,128]{1,0:T(8,128)(2,1)}, u32[]{:S(2)}, u32[]{:S(2)}) collective-permute-start(bf16[8192,128]{1,0:T(8,128)(2,1)} %constant_dynamic-update-slice_fusion.16), channel_id=1, source_target_pairs={{0,128},{4,132},{8,136},{12,140},{16,144},{20,148},{24,152},{28,15... | collective-permute-start | bytes 6291464 | tf_op jit(solution)/shard_map/ppermute | solution.py:13
  433.0 14.7 %copy-start.22 = (f32[2048]{0:T(1024)S(1)}, f32[2048]{0:T(1024)}, u32[]{:S(2)}) copy-start(f32[2048]{0:T(1024)} %param.26) | copy-start | bytes 24580
  434.9 8.7 %all-to-all-start = ((bf16[4,64,256]{2,1,0:T(8,128)(2,1)}), bf16[4,64,256]{2,1,0:T(8,128)(2,1)S(1)}, u32[]{:S(2)}, u32[]{:S(2)}) async-start(bf16[4,64,256]{2,1,0:T(8,128)(2,1)} %copy.141), calls=%async_computation | async-start | bytes 262144 | tf_op jit(solution)/shard_map/all_to_all | solution.py:143
  438.8 150.4 %reduce-scatter.2.cloned.1.call-start = ((), (), s32[]{:S(2)}) async-start(), calls=%async_computation.6 | async-start | bytes 3932160 | tf_op jit(solution)/shard_map/reduce_scatter | solution.py:184
  446.9 0.9 copy-start.5
  496.0 41.0 %copy-start.26 = (bf16[1,2048,768]{2,1,0:T(8,128)(2,1)S(1)}, bf16[1,2048,768]{2,1,0:T(8,128)(2,1)}, u32[]{:S(2)}) copy-start(bf16[1,2048,768]{2,1,0:T(8,128)(2,1)} %param.30) | copy-start | bytes 9437188
  535.3 1.7 copy-start.6
  552.1 82.6 %copy-start.24 = (f32[64,2]{0,1:T(2,128)S(1)}, f32[64,2]{0,1:T(2,128)}, u32[]{:S(2)}) copy-start(f32[64,2]{0,1:T(2,128)} %param.28) | copy-start | bytes 1540
Sparse Core Ops, SparseCore 0:
  13.2 51.5 all-gather.1
  552.2 36.9 reduce-scatter.1
